TPU v7x, 32 devices: a whole 2x2x4 slice. The times are simulated.
32 devices in a mesh: st: 8 (over z, x), tp: 4 (over y, core).
Axes of the slice: x: 2, y: 2, z: 4, core: 2. Of those that a mesh axis runs over, the one named last changes fastest.
Arguments:
- tokens: bfloat16 [4096, 2048], P('st'), may hold values from -6 to 6
- mix_query: bfloat16 [2048, 1024], P(None, 'tp'), may hold values from -0.125 to 0.125
- mix_key: bfloat16 [2048, 1024], P(None, 'tp'), may hold values from -0.125 to 0.125
- mix_value: bfloat16 [2048, 1024], P(None, 'tp'), may hold values from -0.125 to 0.125
- decay_lower_map: bfloat16 [2048, 64], replicated, may hold values from -0.125 to 0.125
- decay_upper_map: bfloat16 [64, 1024], P(None, 'tp'), may hold values from -1 to 1
- decay_base: float32 [1024], P('tp'), may hold values from -7.5 to -2.5
- decay_shift: float32 [4096, 16], P('st', 'tp'), may hold values from -3.8 to 9.8
- rate_lower_map: bfloat16 [2048, 64], replicated, may hold values from -0.125 to 0.125
- rate_upper_map: bfloat16 [64, 1024], P(None, 'tp'), may hold values from -0.75 to 0.75
- norm_gain: float32 [1024], P('tp'), may hold values from 0.1 to 1.9
- mix_out: bfloat16 [1024, 2048], P(None, 'tp'), may hold values from -0.1875 to 0.1875
- cross_query: bfloat16 [2048, 2048], P(None, 'tp'), may hold values from -0.125 to 0.125
- score_gain: float32 [2048], P('tp'), may hold values from 0.1 to 1.9
- passage_key: bfloat16 [2048, 2048], P(None, 'tp'), may hold values from -0.125 to 0.125
- passage_value: bfloat16 [2048, 2048], P(None, 'tp'), may hold values from -0.125 to 0.125
- cross_out: bfloat16 [2048, 2048], P(None, 'tp'), may hold values from -0.5 to 0.5
- gate_down: bfloat16 [2048, 128], replicated, may hold values from -0.125 to 0.125
- gate_up: bfloat16 [128, 2048], P(None, 'tp'), may hold values from -0.5 to 0.5
- store: bfloat16 [96, 96, 2048], P('st'), may hold values from -6 to 6
- passage_ids: int32 [64, 4], P('st'), may hold values from 0 to 95, as said below
Outputs:
- mixed: bfloat16 [4096, 2048], P('st', 'tp')
Inputs may be any that keep to these rules, and one draw needn't show every extreme that they name: `passage_ids`: among the 32 passages named by the rows of one sequence, at most 4 are held by one index of st (passage p by index p // 12); in every draw exactly 4 are held by the index before the sequence's own.
All inputs are finite; a program needn't handle non-finite values.
Results may differ from a plain program's by a relative error of at most 0.0075.
Values may be sent and summed in bfloat16 or wider, within the bound.
A program may use at most 128 MiB of HBM per device.

v0:
```python
import contextlib
import functools

import jax
import jax.numpy as jnp
from jax import lax
from jax.experimental import pallas as pl
from jax.experimental.pallas import tpu as pltpu
from jax.sharding import PartitionSpec as P

XHEAD = 256
QBLOCK = 64
MBLOCK = 64

FLOAT32 = jnp.float32
BFLOAT = jnp.bfloat16
MESH = pl.DeviceIdType.MESH
scope = contextlib.nullcontext
ST, TP = "st", "tp"


def split(values):
    high = values.astype(BFLOAT)
    return high, (values - high.astype(FLOAT32)).astype(BFLOAT)


def raw_dot(left, right, dims=((1,), (0,))):
    return lax.dot_general(left, right, (dims, ((), ())), preferred_element_type=FLOAT32)


def fine_dot(left, right, dims=((1,), (0,))):
    left = left[0] if isinstance(left, tuple) else left.astype(BFLOAT)
    right = right[0] if isinstance(right, tuple) else right.astype(BFLOAT)
    return raw_dot(left, right, dims)


def exact_dot(values, ones):
    return raw_dot(values.astype(BFLOAT), ones)


def iota(shape, dim):
    return lax.broadcasted_iota(jnp.int32, shape, dim)


def each(fn, *lists):
    return [fn(*items) for items in zip(*lists)]


def recur_step(heads, blocks, base, refs, gain, state_ref, out_ref):
    query_ref, key_ref, value_ref, fade_ref, gate_ref = refs
    width = query_ref.shape[1]
    size = width // heads
    rows = heads * MBLOCK
    row_head = (iota((rows, width), 0) // MBLOCK) == (iota((rows, width), 1) // size)
    state_head = (iota((width, width), 0) // size) == (iota((width, width), 1) // size)
    ones_head = jnp.where(state_head, 1.0, 0.0).astype(BFLOAT)
    row_pos = iota((rows, rows), 0) % MBLOCK
    col_pos = iota((rows, rows), 1) % MBLOCK
    strict = col_pos < row_pos
    upto = col_pos <= row_pos
    lower = jnp.where(
        iota((MBLOCK, MBLOCK), 1) <= iota((MBLOCK, MBLOCK), 0), 1.0, 0.0
    ).astype(BFLOAT)

    def expand(values):
        return jnp.where(row_head, jnp.concatenate([values] * heads, axis=0), 0.0)

    def compact(values):
        return jnp.concatenate(
            [values[:, head * size : (head + 1) * size] for head in range(heads)], axis=0
        )

    def natural(values):
        return jnp.concatenate(
            [values[head * MBLOCK : (head + 1) * MBLOCK] for head in range(heads)], axis=1
        )

    def span(block):
        return pl.ds(pl.multiple_of(base + block * MBLOCK, MBLOCK), MBLOCK)

    def load(ref):
        return [ref[span(b), :].astype(FLOAT32) for b in range(blocks)]

    def running_sum(fade):
        high, low = split(fade)
        rest = (fade - high.astype(FLOAT32) - low.astype(FLOAT32)).astype(BFLOAT)
        return raw_dot(lower, high) + (raw_dot(lower, low) + raw_dot(lower, rest))

    query, key, value = load(query_ref), load(key_ref), load(value_ref)
    fade, gate = load(fade_ref), load(gate_ref)
    cumul = each(running_sum, fade)
    unit = each(lambda k: k * lax.rsqrt(exact_dot(k * k, ones_head) + 1e-06), key)
    rate = each(lambda u, g: u * g, unit, gate)
    minus_scaled = each(lambda u, c, f: -u * jnp.exp(c - f), unit, cumul, fade)
    query_scaled = each(lambda q, c: q * jnp.exp(c), query, cumul)
    inverse = each(lambda c: jnp.exp(-c), cumul)
    fade_out = each(lambda c: jnp.exp(c[MBLOCK - 1 :, :] - c), cumul)
    block_fade = each(lambda c: jnp.exp(c[MBLOCK - 1 :, :]), cumul)
    left = each(
        lambda m, q: split(jnp.concatenate([expand(m), expand(q)], axis=0)),
        minus_scaled,
        query_scaled,
    )
    right = each(
        lambda k, r, i: split(jnp.concatenate([expand(k * i), expand(r * i)], axis=0)),
        key,
        rate,
        inverse,
    )
    pairs = each(lambda a, b: fine_dot(a, b, ((1,), (1,))), left, right)
    key_mats = each(
        lambda p: jnp.concatenate(
            [jnp.where(strict, p[:rows, :rows], 0.0), jnp.where(upto, p[rows:, :rows], 0.0)], axis=0
        ),
        pairs,
    )
    rate_pull = each(lambda p: split(jnp.where(strict, p[:rows, rows:], 0.0)), pairs)
    rate_read = each(lambda p: split(jnp.where(upto, p[rows:, rows:], 0.0)), pairs)
    value_rows = each(lambda v: compact(v).astype(BFLOAT), value)

    def key_values(mats, vals):
        return raw_dot(mats.astype(BFLOAT), vals)

    from_values = each(key_values, key_mats, value_rows)
    solved = each(
        lambda m, kv: jnp.concatenate([compact(m), kv[:rows]], axis=1), minus_scaled, from_values
    )
    power = rate_pull
    levels = (MBLOCK - 1).bit_length()
    for level in range(levels):
        solved = each(lambda s, p: s + fine_dot(p, s), solved, power)
        if level < levels - 1:
            power = each(lambda p: split(fine_dot(p, p)), power)
    solved_halves = each(split, solved)
    reads = each(
        lambda q, kv, r, s: jnp.concatenate([compact(q), kv[rows:]], axis=1) + fine_dot(r, s),
        query_scaled,
        from_values,
        rate_read,
        solved_halves,
    )
    moved = each(
        lambda s, r, f: fine_dot(s, expand(r * f), ((0,), (0,))), solved_halves, rate, fade_out
    )

    def key_update(vals, k, f):
        return raw_dot(vals, expand(k * f).astype(BFLOAT), ((0,), (0,)))

    added = each(key_update, value_rows, key, fade_out)
    carry = each(
        lambda m: split(jnp.where(state_head, jnp.concatenate([m[:size]] * heads, axis=0), 0.0)),
        moved,
    )
    added = each(lambda a, m: a + m[size:], added, moved)
    read_state = each(lambda r: split(natural(r[:, :size])), reads)
    read_fixed = each(lambda r: natural(r[:, size:]), reads)
    state = state_ref[...]
    head_out = []
    for block in range(blocks):
        spread_state = jnp.where(state_head, jnp.concatenate([state] * heads, axis=0), 0.0)
        head_out.append(
            read_fixed[block] + fine_dot(read_state[block], spread_state, ((1,), (1,)))
        )
        state = state * block_fade[block] + fine_dot(state, carry[block]) + added[block]
    state_ref[...] = state
    for block in range(blocks):
        mean = exact_dot(head_out[block], ones_head) * (1.0 / size)
        centred = head_out[block] - mean
        variance = exact_dot(centred * centred, ones_head) * (1.0 / size)
        normed = centred * lax.rsqrt(variance + 0.00064) * gain
        out_ref[0, span(block), :] = normed.astype(BFLOAT)


class Names(dict):
    __getattr__ = dict.__getitem__


def remote(src, dst, send, recv, **peer):
    return pltpu.make_async_remote_copy(
        src_ref=src,
        dst_ref=dst,
        send_sem=send,
        recv_sem=recv,
        device_id=peer,
        device_id_type=MESH,
    )


def when(valid, action):
    if valid is True:
        action()
    else:
        pl.when(valid)(action)


def layer_kernel(size, tree, *refs):
    ids, given, big, out, keep = jax.tree.unflatten(tree, refs)
    keep = Names(keep)
    small = Names(keep.small)
    n, tp, depth, wide = size.owners, size.tp, size.depth, size.wide
    lines = tp // 2
    cap, heads, per_block = size.capacity, size.cross_heads, size.per_block
    me = lax.axis_index(ST)
    mine = lax.axis_index(TP)
    level, column = me // wide, me % wide
    half = depth // 2
    upper = level // half
    base = upper * half
    hub = half - 1 + upper
    off_hub = upper * (level - hub) + (1 - upper) * (hub - level)
    hubbed = range(0)

    def seating(head):
        if head in hubbed:
            return base * wide, half * wide
        return 0, n

    line, core = mine // 2, mine % 2
    sibling = line * 2 + 1 - core

    loads = [
        pltpu.make_async_copy(src, dst, keep.load_sem.at[i])
        for i, (src, dst) in enumerate(zip(big, keep.big))
    ]
    (
        load_tokens,
        load_query,
        load_store,
        load_key,
        load_value,
        load_mix_query,
        load_mix_key,
        load_mix_value,
        load_decay,
        load_rate,
        load_gate,
        load_mix_out,
        load_cross,
    ) = loads
    (
        tokens,
        cross_query,
        store,
        passage_key,
        passage_value,
        mix_query,
        mix_key,
        mix_value,
        decay_lower,
        rate_lower,
        gate_down,
        mix_out,
        cross_out,
    ) = keep.big
    little = {
        name: pltpu.make_async_copy(given[name], small[name], keep.small_sem.at[i])
        for i, name in enumerate(given)
    }
    load_tokens.start()
    load_query.start()
    for copy in little.values():
        copy.start()

    barrier = pltpu.get_barrier_semaphore()

    @pl.loop(1, n)
    def _(d):
        pl.semaphore_signal(barrier, inc=1, device_id={ST: (me + d) % n}, device_id_type=MESH)

    for k in range(1, lines):
        peer = ((line + k) % lines) * 2 + core
        pl.semaphore_signal(barrier, inc=1, device_id={TP: peer}, device_id_type=MESH)
    pl.semaphore_signal(barrier, inc=1, device_id={TP: sibling}, device_id_type=MESH)

    slots = size.blocks * per_block
    down_slot = iota((slots, 128), 0)
    lane = iota((slots, 128), 1)
    by_lane = jnp.zeros((slots, 128), jnp.int32)
    by_slot = jnp.zeros((slots, 128), jnp.int32)
    for j in range(slots):
        ident = ids[j % per_block, j // per_block]
        by_lane = jnp.where(lane == j, ident, by_lane)
        by_slot = jnp.where(down_slot == j, ident, by_slot)
    owner_lane, owner_slot = by_lane // size.pass_dev, by_slot // size.pass_dev
    same = owner_lane == owner_slot
    valid = lane < slots

    def count(flags, axis):
        total = jnp.sum(jnp.where(flags & valid, 1, 0), axis=axis, keepdims=True)
        return jnp.minimum(total, cap - 1)

    rank_lane = count(same & (down_slot > lane), 0)
    rank_slot = count(same & (lane > down_slot), 1)
    power = jnp.ones((slots, 1), jnp.int32)
    for s in range(1, cap):
        power = jnp.where(rank_slot == s, 64**s, power)
    mine_too = owner_slot == lane - 64
    code = jnp.sum(jnp.where(mine_too, (down_slot + 1) * power, 0), axis=0, keepdims=True)
    table = jnp.where(lane[:1] < 64, by_lane[:1] * 8 + rank_lane, code)
    keep.names_out[...] = table
    keep.names_in[me] = table

    def name_copy(d):
        return remote(
            keep.names_out,
            keep.names_in.at[me],
            keep.name_send,
            keep.name_recv,
            st=(me + d) % n,
        )

    own_names = pltpu.make_async_copy(keep.names_out, keep.own, keep.own_sem)
    own_names.start()

    above = [(k, level - k >= 0, level - k) for k in range(1, depth)]
    below = [(depth - 1 + k, level + k < depth, level + k) for k in range(1, depth)]
    origins = [(0, True, level)] + above + below

    def dense_copy(head, rel, dst, target):
        return remote(
            keep.dense[head][rel],
            keep.dense[head][dst],
            keep.dense_send[head].at[dst],
            keep.dense_recv[head].at[dst],
            st=target,
        )

    def forwards(head, rel):
        moves = []
        if rel < depth - 1:
            copy = dense_copy(head, rel, rel + 1, (me + wide) % n)
            held = level < depth - 1
            moves.append(((level - rel >= 0) & held if rel else held, copy))
        if rel == 0 or depth - 1 < rel < 2 * depth - 2:
            far = rel - depth + 1 if rel else 0
            copy = dense_copy(head, rel, depth + far, (me + n - wide) % n)
            held = level > 0
            moves.append(((level + far < depth) & held if rel else held, copy))
        return moves

    def side_copy(head, rel, turn):
        slot = rel * wide + turn
        return remote(
            keep.side_out[head].at[slot],
            keep.side_in[head].at[slot],
            keep.side_send[head].at[rel * (wide - 1) + turn - 1],
            keep.side_recv[head].at[rel * (wide - 1) + turn - 1],
            st=level * wide + (column + turn) % wide,
        )

    def digit(code, s):
        return jnp.clip((code // 64**s) % 64 - 1, 0, slots - 1)

    def spread_queries(head, rel, row, where):
        for _, copy in forwards(head, rel):
            pl.when(_)(copy.start)
        for turn in range(1, wide):
            target = where * 0 + level * wide + (column + turn) % wide
            code = row(64 + target)
            for s in range(cap):
                keep.side_out[head][rel * wide + turn, s] = keep.dense[head][rel][
                    digit(code, s) // per_block
                ]
            side_copy(head, rel, turn).start()

    def from_served(source):
        return lambda index: keep.served[source, 0, index]

    for copy in little.values():
        copy.wait()
    load_tokens.wait()
    load_query.wait()
    for copy in loads[2:]:
        copy.start()

    for head in range(heads):
        with scope("q"):
            cols = pl.ds(head * XHEAD, XHEAD)
            dots = raw_dot(tokens[...], cross_query[:, cols])
            mean = jnp.mean(dots * dots, axis=-1, keepdims=True)
            queries = (dots * lax.rsqrt(mean + 1e-06) * small.score_gain[:, cols]).astype(BFLOAT)
            keep.dense[head][0][...] = queries.reshape(keep.dense[head][0].shape)
            if head == 0:
                own_names.wait()
                pl.semaphore_wait(barrier, n - 1 + lines)

                @pl.loop(1, n)
                def _(d):
                    name_copy(d).start()

            if head == 0 or not 0:
                spread_queries(head, 0, lambda index: keep.own[0, index], level)

    with scope("kv"):
        load_store.wait()
        load_key.wait()
        load_value.wait()
        length = size.passage_len
        group = 4 if size.pass_dev % 4 == 0 else 1
        chunk = group * length
        for head in range(heads):
            cols = pl.ds(head * XHEAD, XHEAD)

            @pl.loop(0, size.pass_dev // group)
            def _(i):
                rows = pl.ds(pl.multiple_of(i * chunk, chunk), chunk)
                part = pl.ds(i * group, group)
                shape = (group, length, XHEAD)
                dots = raw_dot(store[rows, :], passage_key[:, cols])
                mean = jnp.mean(dots * dots, axis=-1, keepdims=True)
                kept = (dots * lax.rsqrt(mean + 1e-06)).astype(BFLOAT)
                keep.kept_keys[head][part] = kept.reshape(shape)
                dots = raw_dot(store[rows, :], passage_value[:, cols])
                keep.kept_values[head][part] = dots.astype(BFLOAT).reshape(shape)

    with scope("names"):

        rest = keep.names_in.at[pl.ds(0, n - 1)]
        remote(rest, rest, keep.name_send, keep.name_recv, st=me).wait_recv()
        served = pltpu.make_async_copy(keep.names_in, keep.served, keep.served_sem)
        served.start()
        served.wait()

    ones = jnp.ones((8, length), BFLOAT)

    def result_copies(head, source, target, parts, sums, marks):
        seat = me - seating(head)[0]
        span = pl.ds(seat * cap, cap)
        recv, recv_sums = marks
        return (
            remote(
                keep.parts_out[head].at[source],
                parts.at[span],
                keep.part_send[head],
                recv,
                st=target,
            ),
            remote(
                keep.sums_out[head].at[source],
                sums.at[span],
                keep.sum_send[head],
                recv_sums,
                st=target,
            ),
        )

    def send_direct(head, source):
        marks = keep.part_recv[head], keep.sum_recv[head]
        for copy in result_copies(head, source, source, keep.parts[head], keep.sums[head], marks):
            copy.start()

    def send_to_hub(head, source, far):
        target = hub * wide + source % wide
        parts, sums = keep.hub_parts[head][far - 1], keep.hub_sums[head][far - 1]
        marks = keep.hub_recv[head][far - 1], keep.hub_sum_recv[head][far - 1]
        for copy in result_copies(head, source, target, parts, sums, marks):
            copy.start()

    def keep_at_hub(head, source, far):
        span = pl.ds((me - seating(head)[0]) * cap, cap)
        keep.hub_parts[head][far - 1][span] = keep.parts_out[head][source]
        keep.hub_sums[head][far - 1][span] = keep.sums_out[head][source]

    def attend(head, rel, turn, floor):
        source = floor * wide + (column + wide - turn) % wide
        local = rel == 0 and turn == 0
        row = from_served(source)
        code = row(64 + me)
        for s in range(cap):
            slot = digit(code, s)
            passage = lax.div(row(slot), 8) % size.pass_dev
            kept, vals = keep.kept_keys[head][passage], keep.kept_values[head][passage]
            if turn:
                asked = keep.side_in[head][rel * wide + turn, s]
            else:
                asked = keep.dense[head][rel][slot // per_block]
            scores = raw_dot(asked, kept, ((1,), (1,)))
            expon = jnp.exp(scores * XHEAD ** (-0.5)).astype(BFLOAT)
            result = raw_dot(expon, vals).astype(BFLOAT)
            total = raw_dot(ones, expon, ((1,), (1,)))[:1]
            total = jnp.concatenate([total, jnp.zeros_like(total)], axis=1)
            if local:
                seat = me - seating(head)[0]
                keep.parts[head][seat * cap + s] = result
                keep.sums[head][seat * cap + s] = total
            else:
                keep.parts_out[head][source, s] = result
                keep.sums_out[head][source, s] = total
        if not local and (rel == 0 or head not in hubbed):
            send_direct(head, source)
        elif rel:
            k = rel if rel < depth else rel - depth + 1
            away = floor // half != upper
            if k < half:
                pl.when(jnp.logical_not(away))(functools.partial(send_direct, head, source))
            for step in range(half):
                far = k - step
                if 1 <= far <= half:
                    send = send_to_hub if step or turn else keep_at_hub
                    pl.when(away & (off_hub == step))(functools.partial(send, head, source, far))

    def pass_on(head, k):
        for rel, valid, floor in (origins[k], origins[depth - 1 + k]):

            def arrive(rel=rel, floor=floor):
                dense_copy(head, rel, rel, me).wait_recv()
                spread_queries(head, rel, from_served(floor * wide + column), floor)

            pl.when(valid)(arrive)

    def from_side(head, k, among):
        for rel, valid, floor in (origins[k], origins[depth - 1 + k]) if k else origins[:1]:

            def arrive(rel=rel, floor=floor):
                attend(head, rel, 0, floor)
                for turn in range(1, wide):
                    side_copy(head, rel, turn).wait_recv()
                    attend(head, rel, turn, floor)

            pl.when(among if valid is True else valid & among)(arrive)

    def mixer_inputs():
        for copy in loads[5:10]:
            copy.wait()
        for weight, target in (
            (mix_query, keep.m_query),
            (mix_key, keep.m_key),
            (mix_value, keep.m_value),
        ):
            target[...] = raw_dot(tokens[...], weight[...]).astype(BFLOAT)
        low = jnp.tanh(raw_dot(tokens[...], decay_lower[...], ((1,), (1,)))).astype(BFLOAT)
        pre = small.decay_base[...] + raw_dot(low, small.decay_upper_map[...])
        lanes = iota((size.mix_heads, pre.shape[1]), 1) // (pre.shape[1] // size.mix_heads)
        chosen = iota(lanes.shape, 0) == lanes
        chosen = jnp.where(chosen, 1.0, 0.0).astype(BFLOAT)
        shift = small.decay_shift[...]
        high, middle = split(shift)
        rest = (shift - high.astype(FLOAT32) - middle.astype(FLOAT32)).astype(BFLOAT)
        first = ((0,), (0,))
        pre = pre + (
            raw_dot(high, chosen, first)
            + (raw_dot(middle, chosen, first) + raw_dot(rest, chosen, first))
        )
        keep.m_fade[...] = jax.nn.sigmoid(pre) * (-(2.718281828459045**-0.5))
        low = raw_dot(tokens[...], rate_lower[...], ((1,), (1,))).astype(BFLOAT)
        keep.m_gate[...] = jax.nn.sigmoid(raw_dot(low, small.rate_upper_map[...]))

    blocks = 2 if size.tokens % (2 * MBLOCK) == 0 else 1
    steps = size.tokens // (blocks * MBLOCK)

    def recur(first, last):
        @pl.loop(first, last)
        def _(i):
            recur_step(
                size.mix_heads,
                blocks,
                i * (blocks * MBLOCK),
                (keep.m_query, keep.m_key, keep.m_value, keep.m_fade, keep.m_gate),
                small.norm_gain[...],
                keep.state,
                keep.mixed,
            )

    def tp_copy(buf, send, recv, slot_from, slot_to, peer):
        return remote(
            buf.at[slot_from], buf.at[slot_to], send.at[slot_to], recv.at[slot_to], tp=peer
        )

    def tp_first(buf, send, recv):
        copies = [tp_copy(buf, send, recv, 0, 1, sibling)]
        for k in range(1, lines):
            peer = ((line + k) % lines) * 2 + core
            copies.append(tp_copy(buf, send, recv, 0, 2 * k, peer))
        return copies

    def tp_second(buf, send, recv):
        return [tp_copy(buf, send, recv, 2 * k, 2 * k + 1, sibling) for k in range(1, lines)]

    def origin(slot):
        k, flip = slot // 2, slot % 2
        return ((line + lines - k) % lines) * 2 + (1 - core if flip else core)

    def relay(first, second):
        for copy, forward in zip(first[1:], second):
            copy.wait_recv()
            forward.start()

    def products(buf, weights, stride, offset, acc, fresh):
        width = buf.shape[2]
        total = None if fresh else acc[...]
        for slot in range(tp):
            start = pl.multiple_of(origin(slot) * stride + offset, 128)
            term = raw_dot(buf[slot], weights[pl.ds(start, width), :])
            total = term if total is None else total + term
        acc[...] = total

    def gates():
        load_gate.wait()
        low = raw_dot(tokens[...], gate_down[...]).astype(BFLOAT)
        keep.opened[...] = jax.nn.sigmoid(raw_dot(low, small.gate_up[...]))

    diagonal = iota((QBLOCK, QBLOCK), 0) == iota((QBLOCK, QBLOCK), 1)

    def await_crowd(head, parts, sums, marks):
        low, crowd = seating(head)
        for full, sem in zip((parts, sums), marks):
            rest = full.at[pl.ds(0, (crowd - 1) * cap)]
            remote(rest, rest, sem, sem, st=me).wait_recv()

    def gather(head, entry_of, parts, sums, b):
        low, crowd = seating(head)
        total = jnp.zeros((QBLOCK, XHEAD), FLOAT32)
        row = jnp.zeros((1, 128), FLOAT32)
        for p in range(per_block):
            entry = entry_of(b * per_block + p)
            owner = lax.div(lax.div(entry, 8), size.pass_dev) - low
            inside = (owner >= 0) & (owner < crowd)
            index = jnp.where(inside, owner * cap + lax.rem(entry, 8), crowd * cap)
            total = total + parts[index].astype(FLOAT32)
            row = row + sums[index]
        return total, row

    def hub_copies(head, far):
        target = (hub + far - 2 * far * upper) * wide + column
        return (
            remote(
                keep.hub_out[head][far - 1],
                keep.far_parts[head],
                keep.hub_send[head].at[far - 1],
                keep.far_recv[head].at[0],
                st=target,
            ),
            remote(
                keep.hub_sums_out[head][far - 1],
                keep.far_sums[head],
                keep.hub_sum_send[head].at[far - 1],
                keep.far_recv[head].at[1],
                st=target,
            ),
        )

    def serve_hub(head, far):
        parts, sums = keep.hub_parts[head][far - 1], keep.hub_sums[head][far - 1]
        source = (hub + far - 2 * far * upper) * wide + column

        @pl.when(level == hub)
        def _():
            marks = keep.hub_recv[head][far - 1], keep.hub_sum_recv[head][far - 1]
            await_crowd(head, parts, sums, marks)

            @pl.loop(0, size.blocks)
            def _(b):
                total, row = gather(head, from_served(source), parts, sums, b)
                keep.hub_out[head][far - 1][b] = total.astype(BFLOAT)
                keep.hub_sums_out[head][far - 1][b] = row

            for copy in hub_copies(head, far):
                copy.start()

    def combine(head):
        parts, sums = keep.parts[head], keep.sums[head]
        buf = keep.attended[head]
        with scope("wait"):
            await_crowd(head, parts, sums, (keep.part_recv[head], keep.sum_recv[head]))
            if head in hubbed:
                for copy in hub_copies(head, 1):
                    copy.wait_recv()
        with scope("comb"):

            @pl.loop(0, size.blocks)
            def _(b):
                total, row = gather(head, lambda index: keep.own[0, index], parts, sums, b)
                if head in hubbed:
                    total = total + keep.far_parts[head][b].astype(FLOAT32)
                    row = row + keep.far_sums[head][b]
                inverse = 1.0 / row[:, :QBLOCK]
                column = jnp.sum(jnp.where(diagonal, inverse, 0.0), axis=1, keepdims=True)
                rows = pl.ds(pl.multiple_of(b * QBLOCK, QBLOCK), QBLOCK)
                buf[0, rows, :] = (total * column).astype(BFLOAT)

    every = []

    def tp_start(buf, send, recv):
        first, second = tp_first(buf, send, recv), tp_second(buf, send, recv)
        for copy in first:
            copy.start()
        every.append(first + second)
        return first, second

    def tp_finish(first, second):
        first[0].wait_recv()
        for copy in second:
            copy.wait_recv()

    def tp_attended(head):
        return tp_start(keep.attended[head], keep.att_send[head], keep.att_recv[head])

    keep.state[...] = jnp.zeros_like(keep.state)
    for head in hubbed:
        none = pl.ds(half * wide * cap, 1)
        for parts in (keep.parts[head], *keep.hub_parts[head]):
            parts[none] = jnp.zeros((1, QBLOCK, XHEAD), BFLOAT)
        for sums in (keep.sums[head], *keep.hub_sums[head]):
            sums[none] = jnp.zeros((1, 1, 128), FLOAT32)
    last = heads - 1
    hubs = []

    moves = [(k, head) for k in range(1, depth) for head in range(heads)]
    moves.sort(key=lambda move: move[0] + 0.5 * move[1])
    edge = (level == 0) | (level == depth - 1)
    queues = [
        (edge, [(head, 0) for head in range(heads)], [1,2,2,2,2,0]),
        (jnp.logical_not(edge), [(head, 0) for head in range(heads)], [9,9,9,2,0]),
    ]

    done = 0

    def catch_up(lag=None):
        with scope("side"):
            for among, waiting, lags in queues:
                keep_back = lags[0] if lag is None else lag
                if len(lags) > 1:
                    lags.pop(0)
                if len(waiting) > keep_back:
                    waiting.sort()
                while len(waiting) > keep_back:
                    from_side(*waiting.pop(0), among)

    for k, head in moves:
        if (k, head) not in moves[:2] and done < steps:
            with scope("rec"):
                recur(done, done + 1)
            done += 1
        if (k, head) == moves[-1]:
            if done < steps:
                with scope("rec"):
                    recur(done, steps)
            with scope("mixx"):
                mixer_moves = tp_start(keep.mixed, keep.mix_send, keep.mix_recv)
                gates()
        with scope("pass"):
            pass_on(head, k)
        for _, waiting, _ in queues:
            waiting.append((head, k))
        if k >= half and head in hubbed:
            hubs.append((head, k - half + 1))
        catch_up()
        if (k, head) == moves[0]:
            for other in range(1, heads if 0 else 1):
                spread_queries(other, 0, lambda index: keep.own[0, index], level)
            with scope("mixin"):
                mixer_inputs()
    catch_up(0)
    with scope("relay"):
        relay(*mixer_moves)
    with scope("hub"):
        for job in hubs:
            serve_hub(*job)
    pending = []
    for head in range(last):
        combine(head)
        pending.append(tp_attended(head))
    with scope("mix"):
        load_mix_out.wait()
        load_cross.wait()
        tp_finish(*mixer_moves)
        products(keep.mixed, mix_out, keep.mixed.shape[2], 0, keep.mix_acc, True)
    combine(last)
    pending.append(tp_attended(last))
    with scope("relay"):
        for copies in pending[:last]:
            relay(*copies)
    def settle():
        rest = keep.names_in.at[pl.ds(0, n - 1)]
        remote(rest, rest, keep.name_send, keep.name_recv, st=me).wait_send()
        for head in range(heads):
            for full, sem in ((keep.parts_out, keep.part_send), (keep.sums_out, keep.sum_send)):
                rest = full[head].at[pl.ds(0, n - 1)]
                remote(rest, rest, sem[head], sem[head], st=me).wait_send()

        @pl.when(level == hub)
        def _():
            for head in hubbed:
                for far in range(1, half + 1):
                    for copy in hub_copies(head, far):
                        copy.wait_send()

        for head in range(heads):
            for rel, valid, floor in origins:
                for held, copy in forwards(head, rel):
                    pl.when(held)(copy.wait_send)
                for turn in range(1, wide):
                    when(valid, side_copy(head, rel, turn).wait_send)

    for head in range(heads):
        if head == last:
            with scope("settle"):
                settle()
        with scope("tpx"):
            if head == last:
                relay(*pending[head])
            tp_finish(*pending[head])
        with scope("cross"):
            buf = keep.attended[head]
            products(buf, cross_out, heads * XHEAD, head * XHEAD, keep.cross_acc, head == 0)

    with scope("out"):
        out[...] = (keep.mix_acc[...] + keep.opened[...] * keep.cross_acc[...]).astype(BFLOAT)

    for copies in every:
        for copy in copies:
            copy.wait_send()


def layer(
    tokens,
    mix_query,
    mix_key,
    mix_value,
    decay_lower_map,
    decay_upper_map,
    decay_base,
    decay_shift,
    rate_lower_map,
    rate_upper_map,
    norm_gain,
    mix_out,
    cross_query,
    score_gain,
    passage_key,
    passage_value,
    cross_out,
    gate_down,
    gate_up,
    store,
    passage_ids,
):
    n, tp = lax.axis_size(ST), lax.axis_size(TP)
    rows, model = tokens.shape
    blocks, per_block = passage_ids.shape
    wide = 1
    while n % (2 * wide) == 0 and (2 * wide) ** 2 <= n:
        wide = 2 * wide
    depth = n // wide
    heads = cross_query.shape[1] // XHEAD
    size = Names(
        owners=n,
        tp=tp,
        wide=wide,
        depth=depth,
        tokens=rows,
        blocks=blocks,
        per_block=per_block,
        pass_dev=store.shape[0],
        passage_len=store.shape[1],
        capacity=max(2, -(-(blocks * per_block) // n)),
        cross_heads=heads,
        mix_heads=decay_shift.shape[1],
    )
    cap = size.capacity
    mix_width = mix_query.shape[1]
    out_cols = mix_out.shape[1]
    relatives = 2 * depth - 1
    small = dict(
        decay_upper_map=decay_upper_map,
        decay_base=decay_base.reshape(1, -1),
        decay_shift=decay_shift.T,
        rate_upper_map=rate_upper_map,
        norm_gain=norm_gain.reshape(1, -1),
        score_gain=score_gain.reshape(1, -1),
        gate_up=gate_up,
    )
    big = (
        tokens,
        cross_query,
        store.reshape(-1, model),
        passage_key,
        passage_value,
        mix_query,
        mix_key,
        mix_value,
        decay_lower_map.T,
        rate_lower_map.T,
        gate_down,
        mix_out,
        cross_out,
    )
    dma = pltpu.SemaphoreType.DMA

    def per_head(make, *shape):
        return [make(*shape) for _ in range(heads)]

    def sems(count):
        return [dma((count,)) for _ in range(heads)]

    def per_far(make, *shape):
        return [[make(*shape) for _ in range(half)] for _ in range(0)]

    query_block = (QBLOCK, XHEAD)
    half = depth // 2
    crowd = half * wide
    crowds = [n] * heads
    scratch = dict(
        big=tuple(pltpu.VMEM(array.shape, array.dtype) for array in big),
        load_sem=dma((len(big),)),
        small={name: pltpu.VMEM(array.shape, array.dtype) for name, array in small.items()},
        small_sem=dma((len(small),)),
        own=pltpu.SMEM((1, 128), jnp.int32),
        own_sem=dma,
        served=pltpu.SMEM((n, 1, 128), jnp.int32),
        served_sem=dma,
        names_out=pltpu.VMEM((1, 128), jnp.int32),
        names_in=pltpu.VMEM((n, 1, 128), jnp.int32),
        name_send=dma,
        name_recv=dma,
        dense=[
            [pltpu.VMEM((blocks,) + query_block, BFLOAT) for _ in range(relatives)]
            for _ in range(heads)
        ],
        dense_send=sems(relatives),
        dense_recv=sems(relatives),
        side_out=per_head(pltpu.VMEM, (relatives * wide, cap) + query_block, BFLOAT),
        side_in=per_head(pltpu.VMEM, (relatives * wide, cap) + query_block, BFLOAT),
        side_send=sems(relatives * (wide - 1)),
        side_recv=sems(relatives * (wide - 1)),
        parts_out=per_head(pltpu.VMEM, (n, cap) + query_block, BFLOAT),
        parts=[pltpu.VMEM((c * cap + 1,) + query_block, BFLOAT) for c in crowds],
        part_send=[dma] * heads,
        part_recv=[dma] * heads,
        sums_out=per_head(pltpu.VMEM, (n, cap, 1, 128), FLOAT32),
        sums=[pltpu.VMEM((c * cap + 1, 1, 128), FLOAT32) for c in crowds],
        sum_send=[dma] * heads,
        sum_recv=[dma] * heads,
        hub_parts=per_far(pltpu.VMEM, (crowd * cap + 1,) + query_block, BFLOAT),
        hub_sums=per_far(pltpu.VMEM, (crowd * cap + 1, 1, 128), FLOAT32),
        hub_recv=per_far(dma, (crowd,)),
        hub_sum_recv=per_far(dma, (crowd,)),
        hub_out=per_far(pltpu.VMEM, (blocks,) + query_block, BFLOAT),
        hub_sums_out=per_far(pltpu.VMEM, (blocks, 1, 128), FLOAT32),
        attended=per_head(pltpu.VMEM, (tp, rows, XHEAD), BFLOAT),
        att_send=sems(tp),
        att_recv=sems(tp),
        kept_keys=per_head(pltpu.VMEM, store.shape[:2] + (XHEAD,), BFLOAT),
        kept_values=per_head(pltpu.VMEM, store.shape[:2] + (XHEAD,), BFLOAT),
        m_query=pltpu.VMEM((rows, mix_width), BFLOAT),
        m_key=pltpu.VMEM((rows, mix_width), BFLOAT),
        m_value=pltpu.VMEM((rows, mix_width), BFLOAT),
        m_fade=pltpu.VMEM((rows, mix_width), FLOAT32),
        m_gate=pltpu.VMEM((rows, mix_width), FLOAT32),
        state=pltpu.VMEM((mix_width // size.mix_heads, mix_width), FLOAT32),
        mixed=pltpu.VMEM((tp, rows, mix_width), BFLOAT),
        mix_send=dma((tp,)),
        mix_recv=dma((tp,)),
        opened=pltpu.VMEM((rows, out_cols), FLOAT32),
        mix_acc=pltpu.VMEM((rows, out_cols), FLOAT32),
        cross_acc=pltpu.VMEM((rows, out_cols), FLOAT32),
    )
    out_shape = jax.ShapeDtypeStruct((rows, out_cols), BFLOAT)
    given = (passage_ids.T, small, big)
    leaves, tree = jax.tree.flatten((*given, out_shape, scratch))
    flat = jax.tree.leaves(given)
    spaces = [pltpu.SMEM] + [pl.ANY] * (len(small) + len(big))
    return pl.pallas_call(
        functools.partial(layer_kernel, size, tree),
        in_specs=[pl.BlockSpec(memory_space=space) for space in spaces],
        out_specs=pl.BlockSpec(memory_space=pltpu.VMEM),
        out_shape=out_shape,
        scratch_shapes=leaves[len(flat) + 1 :],
        compiler_params=pltpu.CompilerParams(
            collective_id=0, has_side_effects=True, vmem_limit_bytes=67043328
        ),
    )(*flat)


def solution(mesh):
    placed = (
        P(ST, None),
        P(None, TP),
        P(None, TP),
        P(None, TP),
        P(),
        P(None, TP),
        P(TP),
        P(ST, TP),
        P(),
        P(None, TP),
        P(TP),
        P(None, TP),
        P(None, TP),
        P(TP),
        P(None, TP),
        P(None, TP),
        P(None, TP),
        P(),
        P(None, TP),
        P(ST, None, None),
        P(ST, None),
    )
    return jax.shard_map(layer, mesh=mesh, in_specs=placed, out_specs=P(ST, TP), check_vma=False)
```

profile of v0, /device:TPU:1, one launch (start us, length us, event | category | flops | bytes accessed | tf_op | source)
XLA Modules:
  0.0 92.7 jit_solution(6862078676618619670)
XLA Ops:
  0.0 90.8 %shard_map.199 = bf16[512,512]{1,0:T(8,128)(2,1)} custom-call(s32[4,8]{1,0:T(4,128)} %bitcast.12, f32[1,256]{1,0:T(1,128)} %bitcast.14, f32[4,512]{1,0:T(4,128)} %bitcast.11, bf16[64,256]{1,0:T(8,128)(2,1)} %refs_3_.1, bf16[128,512]{1,0:T(8,128)(2,1)} %refs_4_.1, f32[1,256]{1,0:T(1,128)} %bitcast.15, bf16[64,256]{1,0:T(8,128)(2,1)} %refs_6_.1, ...), custom_call_target="tpu_custom_call" | custom-call | tf_op jit(solution)/shard_map/pallas_call | solution.py:963
  90.8 1.9 %copy.23 = bf16[512,512]{1,0:T(8,128)(2,1)} copy(bf16[512,512]{1,0:T(8,128)(2,1)} %shard_map.199) | data formatting | bytes 1048576
where the time goes:
time: 92.9 us; the launch traced here: 92.7 us
  Pallas kernels  90.8 us (98%)
  local copies, waits for them, and re-layouts  1.87 us (2%)
    pallas_call x1, Pallas kernels, layer(): pl.pallas_call(functools.partial(layer_kernel, size, tree), in_specs=[pl....  90.8 us
    unnamed x1, local copies, waits for them, and re-layouts  1.87 us

commit v1 on v0

--- a/solution.py
+++ b/solution.py
@@ -709,7 +709,7 @@
     moves.sort(key=lambda move: move[0] + 0.5 * move[1])
     edge = (level == 0) | (level == depth - 1)
     queues = [
-        (edge, [(head, 0) for head in range(heads)], [1,2,2,2,2,0]),
+        (edge, [(head, 0) for head in range(heads)], [1,2,2,2,1,0]),
         (jnp.logical_not(edge), [(head, 0) for head in range(heads)], [9,9,9,2,0]),
     ]
 

time: 92.9 us -> 92.9 us (level)
  no operation moved by 1% of the time
where the time goes in v1:
time: 92.9 us; the launch traced here: 92.7 us
  Pallas kernels  90.8 us (98%)
  local copies, waits for them, and re-layouts  1.87 us (2%)
    pallas_call x1, Pallas kernels, layer(): pl.pallas_call(functools.partial(layer_kernel, size, tree), in_specs=[pl....  90.8 us
    unnamed x1, local copies, waits for them, and re-layouts  1.87 us

profile of v1, /device:TPU:1, one launch (start us, length us, event | category | flops | bytes accessed | tf_op | source)
XLA Modules:
  0.0 92.7 jit_solution(3322587102219468875)
XLA Ops:
  0.0 90.8 %shard_map.199 = bf16[512,512]{1,0:T(8,128)(2,1)} custom-call(s32[4,8]{1,0:T(4,128)} %bitcast.12, f32[1,256]{1,0:T(1,128)} %bitcast.14, f32[4,512]{1,0:T(4,128)} %bitcast.11, bf16[64,256]{1,0:T(8,128)(2,1)} %refs_3_.1, bf16[128,512]{1,0:T(8,128)(2,1)} %refs_4_.1, f32[1,256]{1,0:T(1,128)} %bitcast.15, bf16[64,256]{1,0:T(8,128)(2,1)} %refs_6_.1, ...), custom_call_target="tpu_custom_call" | custom-call | tf_op jit(solution)/shard_map/pallas_call | solution.py:963
  90.9 1.9 %copy.23 = bf16[512,512]{1,0:T(8,128)(2,1)} copy(bf16[512,512]{1,0:T(8,128)(2,1)} %shard_map.199) | data formatting | bytes 1048576
